TPU v7x, 32 devices: a whole 2x2x4 slice. The times are simulated.
32 devices in a mesh: sp: 8 (over z, x), tp: 4 (over y, core).
Axes of the slice: x: 2, y: 2, z: 4, core: 2. Of those that a mesh axis runs over, the one named last changes fastest.
Arguments:
- tokens: bfloat16 [4096, 4096], P('sp', 'tp'), may hold values from -8 to 8
- w_key: bfloat16 [4096, 2048], P(None, 'tp'), may hold values from -0.09375 to 0.09375
- w_value: bfloat16 [4096, 2048], P(None, 'tp'), may hold values from -0.09375 to 0.09375
- w_beta: bfloat16 [4096, 16], replicated, may hold values from -0.09375 to 0.09375
- w_decay: bfloat16 [4096, 16], replicated, may hold values from -0.09375 to 0.09375
- beta_bias: float32 [16], replicated, may hold values from -6 to -4
- decay_rate: float32 [16], replicated, as said below
- forgetting_increment: float32 [16, 4096], P('tp', 'sp')
- new_query: bfloat16 [16, 128], P('tp', 'sp'), may hold values from -6 to 6
- read_gain: bfloat16 [128], replicated, may hold values from 0.099609375 to 1.8984375
Outputs:
- state_cache: bfloat16 [16, 128, 128], P('tp', 'sp')
- first_read: float32 [16, 128], P('tp')
Inputs may be any that keep to these rules, and one draw needn't show every extreme that they name: `decay_rate`: positive.
All inputs are finite; a program needn't handle non-finite values.
Results may differ from a plain program's by a relative error of at most 0.0075.
Values may be sent and summed in bfloat16 or wider, within the bound.
A program may use at most 64 MiB of HBM per device.

v0:
```python
import jax
import jax.numpy as jnp
from jax import lax
from jax.sharding import PartitionSpec as P

DK = 128
DV = 128
BLOCK = 64
norm_eps = 1e-06


def prefix(part, axis, combine, identity):
    count = lax.axis_size(axis)
    place = lax.axis_index(axis)
    ahead = count - 1 - place
    gathered = lax.all_gather(part, axis)
    state = jnp.zeros_like(part) + jnp.asarray(identity, part.dtype)

    def one(lap, state):
        source = count - 1 - lap
        return combine(state, lax.dynamic_index_in_dim(gathered, source, 0, False))

    return lax.fori_loop(0, ahead, one, state)


def matmul_f32(left, right):
    return jnp.dot(left, right, precision=lax.Precision.HIGHEST)


def batched_f32(left, right):
    return jnp.einsum("hij,hjk->hik", left, right, precision=lax.Precision.HIGHEST)


def unit_inverse(lower):
    current_size = lower.shape[0]
    identity = jnp.eye(current_size, dtype=jnp.float32)
    result = identity - lower
    lower_power = lower
    covered = 2
    while covered < current_size:
        lower_power = matmul_f32(lower_power, lower_power)
        result = matmul_f32(result, identity + lower_power)
        covered = covered * 2
    return result


def block_terms(key_blk, value_blk, beta_blk, logd_blk):
    current_size = key_blk.shape[0]
    cumulative = jnp.cumsum(logd_blk)
    spread = cumulative[:, None] - cumulative[None, :]
    location_positions = jnp.arange(current_size)
    causal = location_positions[:, None] >= location_positions[None, :]
    strict = location_positions[:, None] > location_positions[None, :]
    decay_table = jnp.where(causal, jnp.exp(jnp.where(causal, spread, 0.0)), 0.0)
    key_beta = key_blk * beta_blk[:, None]
    lower = jnp.where(strict, matmul_f32(key_beta, key_blk.T) * decay_table, 0.0)
    inverse = unit_inverse(lower)
    update = matmul_f32(inverse, value_blk * beta_blk[:, None])
    erase = matmul_f32(inverse, key_beta * jnp.exp(cumulative)[:, None])
    key_remainder = key_blk * jnp.exp(cumulative[-1] - cumulative)[:, None]
    return (update, erase, key_remainder, jnp.exp(cumulative[-1]))


def per_device(
    tokens,
    w_key,
    w_value,
    w_beta,
    w_decay,
    beta_bias,
    decay_rate,
    forgetting_increment,
    new_query,
    read_gain,
):
    heads_here = w_key.shape[1] // DK
    token_count = tokens.shape[0]
    head_start = lax.axis_index("tp") * heads_here
    gate_weights = jnp.concatenate(
        [
            lax.dynamic_slice_in_dim(w_beta, head_start, heads_here, 1),
            lax.dynamic_slice_in_dim(w_decay, head_start, heads_here, 1),
        ],
        axis=1,
    )
    piece = lax.all_gather(tokens, "tp", axis=1, tiled=True)
    key_acc = jnp.dot(piece, w_key, preferred_element_type=jnp.float32)
    value_acc = jnp.dot(piece, w_value, preferred_element_type=jnp.float32)
    gate_acc = jnp.dot(piece, gate_weights, preferred_element_type=jnp.float32)
    key_wide = (
        lax.optimization_barrier(key_acc.astype(jnp.bfloat16))
        .astype(jnp.float32)
        .reshape(token_count, heads_here, DK)
    )
    key_unit = key_wide * lax.rsqrt(jnp.sum(key_wide * key_wide, axis=-1, keepdims=True) + norm_eps)
    value_wide = (
        lax.optimization_barrier(value_acc.astype(jnp.bfloat16))
        .astype(jnp.float32)
        .reshape(token_count, heads_here, DV)
    )
    bias_here = lax.dynamic_slice_in_dim(beta_bias, head_start, heads_here, 0)
    rate_here = lax.dynamic_slice_in_dim(decay_rate, head_start, heads_here, 0)
    beta = jax.nn.sigmoid(gate_acc[:, :heads_here] + bias_here).T
    log_decay = (
        -rate_here[:, None] * jax.nn.softplus(gate_acc[:, heads_here:].T) + forgetting_increment
    )
    blocks = token_count // BLOCK
    key_heads = key_unit.transpose(1, 0, 2).reshape(heads_here, blocks, BLOCK, DK)
    value_heads = value_wide.transpose(1, 0, 2).reshape(heads_here, blocks, BLOCK, DV)
    terms = jax.vmap(jax.vmap(block_terms))(
        key_heads,
        value_heads,
        beta.reshape(heads_here, blocks, BLOCK),
        log_decay.reshape(heads_here, blocks, BLOCK),
    )
    inputs = tuple((jnp.moveaxis(item, 1, 0) for item in terms))
    identity = jnp.broadcast_to(jnp.eye(DK, dtype=jnp.float32), (heads_here, DK, DK))
    value_zeros = jnp.zeros((heads_here, DK, DV), jnp.float32)
    padding = jnp.zeros((heads_here, BLOCK, DK), jnp.float32)

    def advance(state, block_in):
        update, erase, key_remainder, keep = block_in
        fresh = jnp.concatenate([update, padding], axis=-1) - jnp.einsum(
            "hcd,hde->hce", erase, state, precision=lax.Precision.HIGHEST
        )
        state = keep[:, None, None] * state + jnp.einsum(
            "hcd,hce->hde", key_remainder, fresh, precision=lax.Precision.HIGHEST
        )
        return (state, None)

    combined, _ = lax.scan(advance, jnp.concatenate([value_zeros, identity], axis=-1), inputs)
    local_b = combined[:, :, :DV]
    local_left = combined[:, :, DV:]
    later_product = prefix(local_left, "sp", batched_f32, identity)
    summed = lax.psum_scatter(
        batched_f32(later_product, local_b), "sp", scatter_dimension=1, tiled=True
    )
    own_rows = summed.astype(jnp.bfloat16)
    partial_read = jnp.sum(
        new_query.astype(jnp.float32)[:, :, None] * own_rows.astype(jnp.float32), axis=1
    )
    raw_read = lax.psum(partial_read, "sp")
    first_read = (
        raw_read
        * lax.rsqrt(jnp.mean(raw_read * raw_read, axis=-1, keepdims=True) + norm_eps)
        * read_gain.astype(jnp.float32)
    )
    return (own_rows, first_read)


def solution(mesh):
    return jax.shard_map(
        per_device,
        mesh=mesh,
        in_specs=(
            P("sp", "tp"),
            P(None, "tp"),
            P(None, "tp"),
            P(),
            P(),
            P(),
            P(),
            P("tp", "sp"),
            P("tp", "sp"),
            P(),
        ),
        out_specs=(P("tp", "sp", None), P("tp", None)),
        check_vma=False,
    )
```

profile of v0, /device:TPU:0, one launch (start us, length us, event | category | flops | bytes accessed | tf_op | source)
XLA Modules:
  0.0 263.8 jit_solution(13869263426340788410)
XLA Ops:
  11.1 35.6 %all-gather.4.cloned.1.call-done = bf16[512,4096]{1,0:T(8,128)(2,1)} async-done(((bf16[512,1024]{1,0:T(8,128)(2,1)}), bf16[512,4096]{1,0:T(8,128)(2,1)}) %all-gather.4.cloned.1.call-update) | async-done | bytes 4194320 | tf_op jit(solution)/shard_map/all_gather | solution.py:86
  46.8 3.4 %convolution_bitcast_fusion.3 = f32[512,8]{0,1:T(8,128)S(1)} fusion(bf16[512,4096]{1,0:T(8,128)(2,1)} %all-gather.4.cloned.1.call-done, bf16[4096,4]{0,1:T(4,128)(2,1)S(1)} %get-tuple-element.148, bf16[4096,4]{0,1:T(4,128)(2,1)S(1)} %get-tuple-element.149), kind=kOutput, calls=%fused_computation.25 | convolution fusion | flops 33685504 | bytes 4276224 | tf_op jit(solution)/shard_map/dot_general | solution.py:89
  52.9 5.9 %convolution_convert_fusion.1 = bf16[512,512]{1,0:T(8,128)(2,1)S(1)} fusion(bf16[512,4096]{1,0:T(8,128)(2,1)} %all-gather.4.cloned.1.call-done, bf16[4096,512]{1,0:T(8,128)(2,1)} %param.15), kind=kOutput, calls=%fused_computation.24 | convolution fusion | flops 2147745792 | bytes 8912896 | tf_op jit(solution)/shard_map/dot_general | solution.py:87
  58.8 2.3 convolution_convert_fusion
  62.7 2.1 multiply_bitcast_fusion
  64.7 2.7 %fusion.15 = f32[4,8,64,64]{3,2,1,0:T(8,128)S(1)} fusion(f32[4,8,64,128]{3,2,1,0:T(8,128)S(1)} %bitcast.101, f32[4,8,64]{2,1,0:T(8,128)S(1)} %reduce_window_sum.11, f32[4,8,64]{2,1,0:T(8,128)S(1)} %mul.102, pred[64,64]{1,0:T(8,128)(4,1)} %get-tuple-element.150, pred[64,64]{1,0:T(8,128)(4,1)} %get-tuple-element.151), kind=kOutput, calls=%fused_computation.22 | convolution fusion | flops 202244096 | bytes 1597440 | tf_op jit(solution)/shard_map/vmap(vmap())/dot_general | solution.py:27
  72.2 1.4 fusion.23
  79.6 2.6 convolution_bitcast_fusion.1
  83.5 29.7 %while.22 = (s32[]{:T(128)}, f32[4,128,256]{2,1,0:T(8,128)S(1)}, f32[8,4]{1,0:T(8,128)}, f32[8,4,64,128]{3,2,0,1:T(8,128)}, f32[8,4,64,128]{3,2,0,1:T(8,128)S(1)}, /*index=5*/f32[8,4,64,128]{3,2,0,1:T(8,128)}, s32[]{:T(128)}) while((s32[]{:T(128)}, f32[4,128,256]{2,1,0:T(8,128)S(1)}, f32[8,4]{1,0:T(8,128)}, f32[8,4,64,128]{3,2,0,1:T(8,128)}, ...), condition=%wide.region_3.4_spmd, body=%wide.region_2.3_spmd.sunk | while | flops 201654272 | bytes 2752661 | solution.py:131
  84.2 1.3 convolution_subtract_fusion.2
  85.5 1.7 convolution_add_fusion.3
  87.9 1.3 convolution_subtract_fusion.2
  89.2 1.7 convolution_add_fusion.3
  91.6 1.3 convolution_subtract_fusion.2
  92.9 1.7 convolution_add_fusion.3
  96.7 1.7 convolution_add_fusion.3
  100.4 1.7 convolution_add_fusion.3
  104.1 1.7 convolution_add_fusion.3
  107.8 1.7 convolution_add_fusion.3
  111.5 1.7 convolution_add_fusion.3
  114.0 49.2 %all-gather.6.cloned.1.call-done = f32[32,128,128]{2,1,0:T(8,128)} async-done(((f32[4,128,128]{2,1,0:T(8,128)}), f32[32,128,128]{2,1,0:T(8,128)}) %all-gather.6.cloned.1.call-update) | async-done | bytes 2097168 | tf_op jit(solution)/shard_map/all_gather | solution.py:16
  163.2 11.3 %while.23 = (s32[]{:T(128)}, f32[4,128,128]{1,2,0:T(8,128)S(1)}, s32[]{:T(128)}, f32[8,4,128,128]{3,2,1,0:T(8,128)}, s32[]{:T(128)}, /*index=5*/s32[]{:T(128)}, s32[]{:T(128)}, s32[]{:T(128)}) while((s32[]{:T(128)}, f32[4,128,128]{1,2,0:T(8,128)S(1)}, s32[]{:T(128)}, f32[8,4,128,128]{3,2,1,0:T(8,128)}, s32[]{:T(128)}, /*index=5*/s32[]{:T(128)}, ...), condition=%wide.region_5.6_spmd, body=%wide.region_4.5_spmd.sunk | while | flops 100663304 | bytes 1310863 | solution.py:23
  163.3 1.6 convolution_bitcast_fusion.5
  164.9 1.6 convolution_bitcast_fusion.5
  166.5 1.6 convolution_bitcast_fusion.5
  168.1 1.6 convolution_bitcast_fusion.5
  169.7 1.6 convolution_bitcast_fusion.5
  171.3 1.6 convolution_bitcast_fusion.5
  172.9 1.6 convolution_bitcast_fusion.5
  175.9 59.9 %reduce-scatter.2.cloned.1.call-done = f32[4,16,128]{2,1,0:T(8,128)} async-done(((f32[4,128,128]{2,1,0:T(8,128)}), f32[4,16,128]{2,1,0:T(8,128)}) %reduce-scatter.2.cloned.1.call-update) | async-done | bytes 32784 | tf_op jit(solution)/shard_map/reduce_scatter | solution.py:135
  235.7 1.4 multiply_reduce_fusion.1
  237.1 19.4 %psum.7 = f32[4,128]{1,0:T(4,128)S(1)} all-reduce(f32[4,128]{1,0:T(4,128)S(1)} %get-tuple-element.144), channel_id=1, replica_groups=mesh['sp'=8,'tp'=4] {'sp'}, use_global_device_ids=true, to_apply=%region_8.9 | all-reduce | flops 512 | bytes 4096 | tf_op jit(solution)/shard_map/psum | solution.py:142
  (86 shorter events, 35.4 us)
Async XLA Ops:
  7.2 43.0 %copy-start.1 = (f32[4,512]{1,0:T(4,128)S(1)}, f32[4,512]{1,0:T(4,128)}, u32[]{:S(2)}) copy-start(f32[4,512]{1,0:T(4,128)} %param.21) | copy-start | bytes 24580
  7.2 39.6 %all-gather.4.cloned.1.call-start = ((), (), s32[]{:S(2)}) async-start(), calls=%async_computation.1 | async-start | bytes 5242880 | tf_op jit(solution)/shard_map/all_gather | solution.py:86
  7.9 155.3 %all-gather.6.cloned.1.call-start = ((), (), s32[]{:S(2)}) async-start(), calls=%async_computation.3 | async-start | bytes 2359296 | tf_op jit(solution)/shard_map/all_gather | solution.py:16
  52.9 5.9 %copy-start = (bf16[512,4096]{1,0:T(8,128)(2,1)S(1)}, bf16[512,4096]{1,0:T(8,128)(2,1)}, u32[]{:S(2)}) copy-start(bf16[512,4096]{1,0:T(8,128)(2,1)} %all-gather.4.cloned.1.call-done) | copy-start | bytes 12582916
  52.9 5.9 %copy-start.3 = (bf16[4096,512]{1,0:T(8,128)(2,1)S(1)}, bf16[4096,512]{1,0:T(8,128)(2,1)}, u32[]{:S(2)}) copy-start(bf16[4096,512]{1,0:T(8,128)(2,1)} %param.16) | copy-start | bytes 12582916
  113.9 61.9 %copy-start.4 = (bf16[128]{0:T(256)(128)(2,1)S(1)}, bf16[128]{0:T(256)(128)(2,1)}, u32[]{:S(2)}) copy-start(bf16[128]{0:T(256)(128)(2,1)} %param.23) | copy-start | bytes 772
  113.9 61.9 %copy-start.2 = (bf16[4,16]{1,0:T(4,128)(2,1)S(1)}, bf16[4,16]{1,0:T(4,128)(2,1)}, u32[]{:S(2)}) copy-start(bf16[4,16]{1,0:T(4,128)(2,1)} %param.22) | copy-start | bytes 388
  113.9 121.8 %reduce-scatter.2.cloned.1.call-start = ((), (), s32[]{:S(2)}) async-start(), calls=%async_computation.2 | async-start | bytes 294912 | tf_op jit(solution)/shard_map/reduce_scatter | solution.py:135
Sparse Core Ops, SparseCore 0:
  9.5 37.1 all-gather.3
  114.1 49.0 all-gather.5
  175.9 59.7 reduce-scatter.1
where the time goes:
time: 265 us; the launch traced here: 264 us
  waiting for transfers between devices  145 us (55%)
  matrix products  66.4 us (25%)
  blocking collectives  19.4 us (7%)
  between operations  14 us (5%)
  local copies, waits for them, and re-layouts  9.67 us (4%)
  other arithmetic  8.34 us (3%)
    reduce_scatter x1, waiting for transfers between devices, per_device(): lax.psum_scatter(batched_f32(later_product, local_b), 'sp', scatter_dimen...  59.9 us
    all_gather x1, waiting for transfers between devices, prefix(): gathered = lax.all_gather(part, axis)  49.2 us
    all_gather x1, waiting for transfers between devices, per_device(): piece = lax.all_gather(tokens, 'tp', axis=1, tiled=True)  35.6 us
    psum x1, blocking collectives, per_device(): raw_read = lax.psum(partial_read, 'sp')  19.4 us
    dot_general x13, matrix products, matmul_f32(): return jnp.dot(left, right, precision=lax.Precision.HIGHEST)  18.7 us
    dot_general x8, matrix products, advance(): jnp.einsum('hcd,hce->hde', key_remainder, fresh, precision=lax.Precision....  13.2 us
    dot_general x8, matrix products, batched_f32(): jnp.einsum('hij,hjk->hik', left, right, precision=lax.Precision.HIGHEST)  12.2 us
    dot_general x8, matrix products, advance(): jnp.einsum('hcd,hde->hce', erase, state, precision=lax.Precision.HIGHEST)  10.7 us
  transfers between devices with their start and end apart: 3, of which 3 were waited for; matrix products, arithmetic and copies ran while one was open for 1% of the time, Pallas kernels for 0%

commit v1 on v0

--- a/solution.py
+++ b/solution.py
@@ -7,6 +7,22 @@
 DV = 128
 BLOCK = 64
 norm_eps = 1e-06
+
+
+def number_members_all_up(block_here):
+    num = lax.axis_size("tp")
+    cards = [(k0, (k0 + 1) % num) for k0 in range(num)]
+
+    def corner_solve(prior):
+        if len(prior) == num:
+            return prior
+        k_now = corner_solve([lax.ppermute(prior[0], "tp", cards), *prior])
+        return k_now
+
+    then = corner_solve([block_here])
+    kept_arr = jnp.concatenate(then, axis=1)
+    base_arr = jnp.roll(kept_arr, (lax.axis_index("tp") + 1) * block_here.shape[1], axis=1)
+    return base_arr
 
 
 def prefix(part, axis, combine, identity):
@@ -83,7 +99,7 @@
         ],
         axis=1,
     )
-    piece = lax.all_gather(tokens, "tp", axis=1, tiled=True)
+    piece = number_members_all_up(tokens)
     key_acc = jnp.dot(piece, w_key, preferred_element_type=jnp.float32)
     value_acc = jnp.dot(piece, w_value, preferred_element_type=jnp.float32)
     gate_acc = jnp.dot(piece, gate_weights, preferred_element_type=jnp.float32)

time: 265 us -> 271 us (1.023)
  waiting for transfers between devices: 145 us -> 152 us
  matrix products: 66.4 us -> 63.3 us
  local copies, waits for them, and re-layouts: 9.67 us -> 12.5 us
    ppermute x0 -> x3, waiting for transfers between devices: none -> 40.9 us  [corner_solve(): k_now = corner_solve([lax.ppermute(prior[0], 'tp', cards), *prior])]
    all_gather x1 -> x0, waiting for transfers between devices: 35.6 us -> none  [per_device(): piece = lax.all_gather(tokens, 'tp', axis=1, tiled=True)]
    unnamed x11 -> x24, local copies, waits for them, and re-layouts: 0.11 us -> 8.84 us
    mul x8, local copies, waits for them, and re-layouts: 5.46 us -> 0.08 us  [advance(): keep[:, None, None] * state]
  transfers between devices with their start and end apart: 3 -> 5, of which waited for: 3 -> 5; matrix products, arithmetic and copies ran while one was open for 1% -> 1% of each run, Pallas kernels for 0% -> 0%
where the time goes in v1:
time: 271 us; the launch traced here: 270 us
  waiting for transfers between devices  152 us (56%)
  matrix products  63.3 us (23%)
  blocking collectives  19.5 us (7%)
  between operations  14.4 us (5%)
  local copies, waits for them, and re-layouts  12.5 us (5%)
  other arithmetic  6.52 us (2%)
    reduce_scatter x1, waiting for transfers between devices, per_device(): lax.psum_scatter(batched_f32(later_product, local_b), 'sp', scatter_dimen...  59.9 us
    all_gather x1, waiting for transfers between devices, prefix(): gathered = lax.all_gather(part, axis)  51.2 us
    ppermute x3, waiting for transfers between devices, corner_solve(): k_now = corner_solve([lax.ppermute(prior[0], 'tp', cards), *prior])  40.9 us
    psum x1, blocking collectives, per_device(): raw_read = lax.psum(partial_read, 'sp')  19.5 us
    dot_general x13, matrix products, matmul_f32(): return jnp.dot(left, right, precision=lax.Precision.HIGHEST)  17.9 us
    dot_general x8, matrix products, advance(): jnp.einsum('hcd,hce->hde', key_remainder, fresh, precision=lax.Precision....  13.2 us
    dot_general x8, matrix products, batched_f32(): jnp.einsum('hij,hjk->hik', left, right, precision=lax.Precision.HIGHEST)  12.2 us
    dot_general x8, matrix products, advance(): jnp.einsum('hcd,hde->hce', erase, state, precision=lax.Precision.HIGHEST)  10.7 us
  transfers between devices with their start and end apart: 5, of which 5 were waited for; matrix products, arithmetic and copies ran while one was open for 1% of the time, Pallas kernels for 0%

profile of v1, /device:TPU:0, one launch (start us, length us, event | category | flops | bytes accessed | tf_op | source)
XLA Modules:
  0.0 269.6 jit_solution(5950774154429114380)
XLA Ops:
  7.8 14.6 %collective-permute-done = bf16[512,1024]{1,0:T(8,128)(2,1)S(1)} collective-permute-done((bf16[512,1024]{1,0:T(8,128)(2,1)}, bf16[512,1024]{1,0:T(8,128)(2,1)S(1)}, u32[]{:S(2)}, u32[]{:S(2)}) %collective-permute-start) | collective-permute-done | bytes 1048608 | tf_op jit(solution)/shard_map/ppermute | solution.py:19
  22.4 14.3 %collective-permute-done.1 = bf16[512,1024]{1,0:T(8,128)(2,1)} collective-permute-done((bf16[512,1024]{1,0:T(8,128)(2,1)S(1)}, bf16[512,1024]{1,0:T(8,128)(2,1)}, u32[]{:S(2)}, u32[]{:S(2)}) %collective-permute-start.1) | collective-permute-done | bytes 1048608 | tf_op jit(solution)/shard_map/ppermute | solution.py:19
  39.3 11.9 %collective-permute-done.2 = bf16[512,1024]{1,0:T(8,128)(2,1)} collective-permute-done((bf16[512,1024]{1,0:T(8,128)(2,1)}, bf16[512,1024]{1,0:T(8,128)(2,1)}, u32[]{:S(2)}, u32[]{:S(2)}) %collective-permute-start.2) | collective-permute-done | bytes 1048608 | tf_op jit(solution)/shard_map/ppermute | solution.py:19
  57.0 3.2 %copy-done.1 = bf16[512,8192]{1,0:T(8,128)(2,1)} copy-done((bf16[512,8192]{1,0:T(8,128)(2,1)}, bf16[512,8192]{1,0:T(8,128)(2,1)S(1)}, u32[]{:S(2)}) %copy-start.1) | copy-done | bytes 8388632
  62.8 5.8 %fusion.24 = bf16[512,512]{1,0:T(8,128)(2,1)S(1)} fusion(bf16[4096,512]{1,0:T(8,128)(2,1)} %param.15, bf16[512,8192]{1,0:T(8,128)(2,1)} %copy-done.1, s32[]{:T(128)S(6)} %select_n.42), kind=kOutput, calls=%fused_computation.29 | convolution fusion | flops 2147745792 | bytes 8912900 | tf_op jit(solution)/shard_map/dot_general | solution.py:103
  70.2 1.9 fusion.21
  79.4 1.4 fusion.33
  83.2 2.3 fusion.27
  86.9 2.6 convolution_bitcast_fusion.1
  92.1 24.5 %while.22 = (s32[]{:T(128)}, f32[4,128,256]{2,1,0:T(8,128)S(1)}, f32[8,4]{1,0:T(8,128)S(1)}, f32[8,4,64,128]{3,2,0,1:T(8,128)}, f32[8,4,64,128]{3,2,0,1:T(8,128)S(1)}, /*index=5*/f32[8,4,64,128]{3,2,0,1:T(8,128)}, s32[]{:T(128)}) while((s32[]{:T(128)}, f32[4,128,256]{2,1,0:T(8,128)S(1)}, f32[8,4]{1,0:T(8,128)S(1)}, ...), condition=%wide.region_3.4_spmd, body=%wide.region_2.3_spmd.sunk | while | flops 201654272 | bytes 2753669 | solution.py:147
  92.1 1.3 convolution_subtract_fusion.2
  93.4 1.7 convolution_add_fusion.3
  96.5 1.7 convolution_add_fusion.3
  98.2 1.3 convolution_subtract_fusion.2
  99.6 1.7 convolution_add_fusion.3
  102.6 1.7 convolution_add_fusion.3
  105.7 1.7 convolution_add_fusion.3
  108.7 1.7 convolution_add_fusion.3
  111.8 1.7 convolution_add_fusion.3
  114.9 1.7 convolution_add_fusion.3
  117.3 51.2 %all-gather.3.cloned.1.call-done = f32[32,128,128]{2,1,0:T(8,128)} async-done(((f32[4,128,128]{2,1,0:T(8,128)}), f32[32,128,128]{2,1,0:T(8,128)}) %all-gather.3.cloned.1.call-update) | async-done | bytes 2097168 | tf_op jit(solution)/shard_map/all_gather | solution.py:32
  168.6 11.3 %while.23 = (s32[]{:T(128)}, f32[4,128,128]{1,2,0:T(8,128)S(1)}, s32[]{:T(128)}, f32[8,4,128,128]{3,2,1,0:T(8,128)}, s32[]{:T(128)}, /*index=5*/s32[]{:T(128)}, s32[]{:T(128)}, s32[]{:T(128)}) while((s32[]{:T(128)}, f32[4,128,128]{1,2,0:T(8,128)S(1)}, s32[]{:T(128)}, f32[8,4,128,128]{3,2,1,0:T(8,128)}, s32[]{:T(128)}, /*index=5*/s32[]{:T(128)}, ...), condition=%wide.region_5.6_spmd, body=%wide.region_4.5_spmd.sunk | while | flops 100663304 | bytes 1310855 | solution.py:39
  168.6 1.6 convolution_bitcast_fusion.4
  170.3 1.6 convolution_bitcast_fusion.4
  171.9 1.6 convolution_bitcast_fusion.4
  173.5 1.6 convolution_bitcast_fusion.4
  175.1 1.6 convolution_bitcast_fusion.4
  176.7 1.6 convolution_bitcast_fusion.4
  178.3 1.6 convolution_bitcast_fusion.4
  181.3 59.9 %reduce-scatter.2.cloned.1.call-done = f32[4,16,128]{2,1,0:T(8,128)} async-done(((f32[4,128,128]{2,1,0:T(8,128)}), f32[4,16,128]{2,1,0:T(8,128)}) %reduce-scatter.2.cloned.1.call-update) | async-done | bytes 32784 | tf_op jit(solution)/shard_map/reduce_scatter | solution.py:151
  241.1 1.4 multiply_reduce_fusion.1
  242.5 19.5 %psum.7 = f32[4,128]{1,0:T(4,128)S(1)} all-reduce(f32[4,128]{1,0:T(4,128)S(1)} %get-tuple-element.144), channel_id=1, replica_groups=mesh['sp'=8,'tp'=4] {'sp'}, use_global_device_ids=true, to_apply=%region_8.9 | all-reduce | flops 512 | bytes 4096 | tf_op jit(solution)/shard_map/psum | solution.py:158
  (104 shorter events, 37.7 us)
Async XLA Ops:
  7.2 46.9 %copy-start = (bf16[512,1024]{1,0:T(8,128)(2,1)S(1)}, bf16[512,1024]{1,0:T(8,128)(2,1)}, u32[]{:S(2)}) copy-start(bf16[512,1024]{1,0:T(8,128)(2,1)} %param.14) | copy-start | bytes 3145732
  7.2 161.4 %all-gather.3.cloned.1.call-start = ((), (), s32[]{:S(2)}) async-start(), calls=%async_computation.2 | async-start | bytes 2359296 | tf_op jit(solution)/shard_map/all_gather | solution.py:32
  7.2 15.2 %collective-permute-start = (bf16[512,1024]{1,0:T(8,128)(2,1)}, bf16[512,1024]{1,0:T(8,128)(2,1)S(1)}, u32[]{:S(2)}, u32[]{:S(2)}) collective-permute-start(bf16[512,1024]{1,0:T(8,128)(2,1)} %param.14), channel_id=1, source_target_pairs={{0,1},{1,2},{2,3},{3,0},{4,5},{5,6},{6,7},{7,4},{8,9},{9,10},{10,1... | collective-permute-start | bytes 3145736 | tf_op jit(solution)/shard_map/ppermute | solution.py:19
  22.4 14.3 %collective-permute-start.1 = (bf16[512,1024]{1,0:T(8,128)(2,1)S(1)}, bf16[512,1024]{1,0:T(8,128)(2,1)}, u32[]{:S(2)}, u32[]{:S(2)}) collective-permute-start(bf16[512,1024]{1,0:T(8,128)(2,1)S(1)} %collective-permute-done), channel_id=1, source_target_pairs={{0,1},{1,2},{2,3},{3,0},{4,5},{5,6},{6,7},{7,4},{8,9},{9,10},{10,1... | collective-permute-start | bytes 3145736 | tf_op jit(solution)/shard_map/ppermute | solution.py:19
  36.7 14.5 %collective-permute-start.2 = (bf16[512,1024]{1,0:T(8,128)(2,1)}, bf16[512,1024]{1,0:T(8,128)(2,1)}, u32[]{:S(2)}, u32[]{:S(2)}) collective-permute-start(bf16[512,1024]{1,0:T(8,128)(2,1)} %collective-permute-done.1), channel_id=1, source_target_pairs={{0,1},{1,2},{2,3},{3,0},{4,5},{5,6},{6,7},{7,4},{8,9},{9,10},{10,1... | collective-permute-start | bytes 3145736 | tf_op jit(solution)/shard_map/ppermute | solution.py:19
  53.9 7.4 %copy-start.2 = (f32[4,512]{1,0:T(4,128)S(1)}, f32[4,512]{1,0:T(4,128)}, u32[]{:S(2)}) copy-start(f32[4,512]{1,0:T(4,128)} %param.21) | copy-start | bytes 24580
  56.9 3.2 %copy-start.1 = (bf16[512,8192]{1,0:T(8,128)(2,1)}, bf16[512,8192]{1,0:T(8,128)(2,1)S(1)}, u32[]{:S(2)}) copy-start(bf16[512,8192]{1,0:T(8,128)(2,1)S(1)} %constant_dynamic-update-slice_fusion) | copy-start | bytes 25165828
  77.0 6.2 %slice-start = ((s8[8388608]{0:T(1024)(128)(4,1)}), s8[4194304]{0:T(1024)(128)(4,1)S(1)}, s32[]{:S(2)}) async-start(s8[8388608]{0:T(1024)(128)(4,1)} %bitcast.100), calls=%async_computation.3 | async-start | bytes 8388608
  77.0 6.2 %copy-start.4 = (bf16[4096,512]{1,0:T(8,128)(2,1)S(1)}, bf16[4096,512]{1,0:T(8,128)(2,1)}, u32[]{:S(2)}) copy-start(bf16[4096,512]{1,0:T(8,128)(2,1)} %param.16) | copy-start | bytes 12582916
  79.4 3.8 %slice-start.1 = ((s8[8388608]{0:T(1024)(128)(4,1)}), s8[4194304]{0:T(1024)(128)(4,1)S(1)}, s32[]{:S(2)}) async-start(s8[8388608]{0:T(1024)(128)(4,1)} %bitcast.100), calls=%async_computation.4 | async-start | bytes 8388608
  92.1 89.2 %copy-start.3 = (bf16[4,16]{1,0:T(4,128)(2,1)S(1)}, bf16[4,16]{1,0:T(4,128)(2,1)}, u32[]{:S(2)}) copy-start(bf16[4,16]{1,0:T(4,128)(2,1)} %param.22) | copy-start | bytes 388
  92.1 89.2 %copy-start.5 = (bf16[128]{0:T(256)(128)(2,1)S(1)}, bf16[128]{0:T(256)(128)(2,1)}, u32[]{:S(2)}) copy-start(bf16[128]{0:T(256)(128)(2,1)} %param.23) | copy-start | bytes 772
  117.3 123.8 %reduce-scatter.2.cloned.1.call-start = ((), (), s32[]{:S(2)}) async-start(), calls=%async_computation.1 | async-start | bytes 294912 | tf_op jit(solution)/shard_map/reduce_scatter | solution.py:151
Sparse Core Ops, SparseCore 0:
  117.4 51.1 all-gather.2
  181.3 59.7 reduce-scatter.1
